TPU v7x, 32 devices: a whole 2x2x4 slice. The times are simulated.
32 devices in a mesh: sp: 16 (over z, y, core), tp: 2 (over x).
Axes of the slice: x: 2, y: 2, z: 4, core: 2. Of those that a mesh axis runs over, the one named last changes fastest.
Arguments:
- queries: bfloat16 [8192, 1024], P('sp', 'tp'), may hold values from -40 to 40
- keys_values: bfloat16 [8192, 4, 128], P('sp', 'tp'), may hold values from -40 to 40
- doc_ids: int32 [8192], P('sp'), may hold values from 0 to 3, never falling along the last dimension, each value on 1 to 4096 neighbouring positions
- head_sink: float32 [16], P('tp'), may hold values from 3 to 7
- out_weight: bfloat16 [1024, 2048], replicated, may hold values from -0.1875 to 0.1875
- hidden_in: bfloat16 [8192, 2048], P(('sp', 'tp')), may hold values from -0.59765625 to 0.59765625
- norm_gain: float32 [2048], replicated, may hold values from 0.1 to 1.9
- expert_gate: bfloat16 [32, 2048, 1024], P(('sp', 'tp')), may hold values from -0.125 to 0.125
- expert_up: bfloat16 [32, 2048, 1024], P(('sp', 'tp')), may hold values from -0.125 to 0.125
- expert_down: bfloat16 [32, 1024, 2048], P(('sp', 'tp')), may hold values from -0.1875 to 0.1875
- routes: int32 [8192, 2], P(('sp', 'tp')), may hold values from 0 to 31, all different within a row; in each aligned block of 256 rows (0 to 255, 256 to 511, ...) at most 32 rows name the same one
- route_weight: float32 [8192, 2], P(('sp', 'tp')), may hold values from 0.1 to 1
Outputs:
- layer_out: bfloat16 [8192, 2048], P(('sp', 'tp'))
Inputs may be any that keep to these rules, and one draw needn't show every extreme that they name: `routes`: in the rows of one device (aligned blocks of 256 tokens in order) no expert is named more than 32 times; some expert is named exactly 32 times in some blocks.
All inputs are finite; a program needn't handle non-finite values.
Results may differ from a plain program's by a relative error of at most 0.02.
Values may be sent and summed in bfloat16 or wider, within the bound.
A program may use at most 64 MiB of HBM per device.

v0:
```python
import jax
import jax.numpy as jnp
from jax import lax
from jax.sharding import PartitionSpec as P

HD = 64
WIN = 128


def with_halo(cells, sides, width):
    for axis, dim in sides:
        count = lax.axis_size(axis)
        ends = count - 1
        head = lax.slice_in_dim(cells, 0, width, axis=dim)
        tail = lax.slice_in_dim(cells, cells.shape[dim] - width, cells.shape[dim], axis=dim)
        cells = jnp.concatenate(
            [
                lax.ppermute(tail, axis, [(i, (i + 1) % count) for i in range(ends)]),
                cells,
                lax.ppermute(head, axis, [((i + 1) % count, i) for i in range(ends)]),
            ],
            axis=dim,
        )
    return cells


def expert_rows(arrived, gate_w, up_w, down_w):
    width = arrived.shape[-1]
    flat_rows = arrived.reshape(-1, width)
    gate = jnp.dot(flat_rows, gate_w, preferred_element_type=jnp.float32)
    upper = jnp.dot(flat_rows, up_w, preferred_element_type=jnp.float32)
    expert_hidden = (jax.nn.silu(gate) * upper).astype(jnp.bfloat16)
    result = jnp.dot(expert_hidden, down_w, preferred_element_type=jnp.float32).astype(jnp.bfloat16)
    return result.reshape(arrived.shape[:-1] + (result.shape[-1],))


def shards(
    queries,
    keys_values,
    doc_ids,
    head_sink,
    out_weight,
    hidden_in,
    norm_gain,
    expert_gate,
    expert_up,
    expert_down,
    routes,
    route_weight,
):
    tok_here = queries.shape[0]
    heads_here = head_sink.shape[0]
    kv_here = keys_values.shape[1]
    group = heads_here // kv_here
    head_dim = keys_values.shape[2] // 2
    kv_ext, docs_ext = (
        with_halo(keys_values, (("sp", 0),), WIN),
        with_halo(doc_ids, (("sp", 0),), WIN),
    )
    offset = lax.axis_index("sp") * tok_here
    seq_total = lax.axis_size("sp") * tok_here
    span_rows = min(512, tok_here)
    sink_logit = head_sink.reshape(kv_here, group)[:, :, None, None]

    def one_span(span_index):
        first_row = span_index * span_rows
        q_span = queries.reshape(span_rows, kv_here, group, head_dim)
        scores = jnp.einsum(
            "qhgd,khd->hgqk", q_span, kv_ext[..., :head_dim], preferred_element_type=jnp.float32
        ) * HD ** (-0.5)
        query_pos = offset + first_row + jnp.arange(span_rows, dtype=jnp.int32)
        key_pos = offset + first_row - WIN + jnp.arange(span_rows + 2 * WIN, dtype=jnp.int32)
        inside = (key_pos >= 0) & (key_pos < seq_total)
        allowed = (
            (jnp.abs(key_pos[None, :] - query_pos[:, None]) <= WIN)
            & inside[None, :]
            & (docs_ext[None, :] == doc_ids[:, None])
        )
        masked = jnp.where(allowed, scores, -1e30)
        row_max = jnp.maximum(masked.max(-1, keepdims=True), sink_logit)
        exp_scores = jnp.where(allowed, jnp.exp(masked - row_max), 0.0)
        total_mass = exp_scores.sum(-1, keepdims=True) + jnp.exp(sink_logit - row_max)
        weights = (exp_scores / total_mass).astype(jnp.bfloat16)
        outcome = jnp.einsum(
            "hgqk,khd->qhgd", weights, kv_ext[..., head_dim:], preferred_element_type=jnp.float32
        )
        return outcome.astype(jnp.bfloat16).reshape(span_rows, heads_here * head_dim)

    attended = lax.map(one_span, jnp.arange(tok_here // span_rows, dtype=jnp.int32)).reshape(
        tok_here, -1
    )
    gathered = lax.all_to_all(attended, "tp", split_axis=0, concat_axis=1, tiled=True)
    projected = jnp.dot(gathered, out_weight, preferred_element_type=jnp.float32)
    mid_wide = (hidden_in.astype(jnp.float32) + projected).astype(jnp.bfloat16).astype(jnp.float32)
    normed = (
        mid_wide
        * lax.rsqrt(jnp.mean(mid_wide * mid_wide, axis=-1, keepdims=True) + 1e-06)
        * norm_gain
    ).astype(jnp.bfloat16)
    local_rows = normed.shape[0]
    topk = routes.shape[1]
    width = normed.shape[1]
    sp_count = lax.axis_size("sp")
    tp_count = lax.axis_size("tp")
    expert_count = sp_count * tp_count
    capacity = 2 * local_rows * topk // expert_count
    flat_routes = routes.reshape(-1)
    one_hot = (flat_routes[:, None] == jnp.arange(expert_count, dtype=jnp.int32)[None, :]).astype(
        jnp.int32
    )
    slot_rank = (jnp.cumsum(one_hot, axis=0) * one_hot).sum(-1) - 1
    slot_index = flat_routes * capacity + slot_rank
    repeated = jnp.repeat(normed, topk, axis=0)
    buffer_rows = (
        jnp.zeros((expert_count * capacity, width), jnp.bfloat16).at[slot_index].set(repeated)
    )
    sent = buffer_rows.reshape(expert_count, capacity, width)
    finished = expert_rows(
        lax.all_to_all(sent, ("sp", "tp"), split_axis=0, concat_axis=0, tiled=True),
        expert_gate[0],
        expert_up[0],
        expert_down[0],
    )
    returned = lax.all_to_all(finished, ("sp", "tp"), split_axis=0, concat_axis=0, tiled=True)
    returned = returned.reshape(expert_count * capacity, width)
    picked = returned[slot_index].astype(jnp.float32).reshape(local_rows, topk, width)
    mixture = jnp.sum(picked * route_weight[..., None], axis=1)
    return (mid_wide + mixture).astype(jnp.bfloat16)


def solution(mesh):
    placed = (
        P("sp", "tp"),
        P("sp", "tp", None),
        P("sp"),
        P("tp"),
        P(),
        P(("sp", "tp"), None),
        P(),
        P(("sp", "tp"), None, None),
        P(("sp", "tp"), None, None),
        P(("sp", "tp"), None, None),
        P(("sp", "tp"), None),
        P(("sp", "tp"), None),
    )
    return jax.shard_map(
        shards, mesh=mesh, in_specs=placed, out_specs=P(("sp", "tp"), None), check_vma=False
    )
```

profile of v0, /device:TPU:0, one launch (start us, length us, event | category | flops | bytes accessed | tf_op | source)
XLA Modules:
  0.0 292.3 jit_solution(11387573325899256415)
XLA Ops:
  0.8 2.4 collective-permute-start.2
  3.2 1.3 collective-permute-start.3
  5.6 5.2 %collective-permute-start = (bf16[128,2,128]{0,2,1:T(8,128)(2,1)S(1)}, bf16[128,2,128]{0,2,1:T(8,128)(2,1)S(1)}, u32[]{:S(2)}, u32[]{:S(2)}) collective-permute-start(bf16[128,2,128]{0,2,1:T(8,128)(2,1)S(1)} %get-tuple-element.19), channel_id=1, source_target_pairs={{0,2},{2,4},{4,6},{6,8},{8,10},{10,12},{12,14},{14,16},{16,18},{18... | collective-permute-start | bytes 196616 | tf_op jit(solution)/shard_map/ppermute | solution.py:18
  10.8 1.3 collective-permute-start.1
  18.1 1.5 fusion.22
  19.8 2.1 fusion
  21.9 3.1 %fusion.1 = f32[2,4,512]{2,1,0:T(4,128)S(1)} fusion(f32[2,768,512,4]{2,1,3,0:T(8,128)S(1)} %get-tuple-element.32, f32[2,4,512]{2,1,0:T(4,128)S(1)} %broadcast_maximum_fusion, pred[512,768]{0,1:T(8,128)(4,1)S(1)} %fusion.22), kind=kLoop, calls=%fused_computation.6 | loop fusion | flops 15724544 | bytes 13008896 | tf_op jit(solution)/shard_map/while/body/eval_jaxpr/reduce_sum | solution.py:82
  25.1 3.9 %fusion.24 = bf16[512,2,4,64]{0,3,2,1:T(8,128)(2,1)S(1)} fusion(f32[2,768,512,4]{2,1,3,0:T(8,128)S(1)} %get-tuple-element.32, f32[2,4,512]{2,1,0:T(4,128)S(1)} %exponential_add_fusion, f32[2,4,512]{2,1,0:T(4,128)S(1)} %broadcast_maximum_fusion, pred[512,768]{0,1:T(8,128)(4,1)S(1)} %fusion.22, bf16[768,2,128]{0,2,1:T(8,128)(2,1)S(1)} %pad_maximum_fusion), kind=kOutput, calls=%fused_computation.32 | convolution fusion | flops 421789696 | bytes 13729792 | tf_op jit(solution)/shard_map/while/body/eval_jaxpr/hgqk,khd->qhgd/dot_general | solution.py:84
  30.0 3.7 %all-to-all-start = ((bf16[2,256,512]{1,2,0:T(8,128)(2,1)}), bf16[2,256,512]{1,2,0:T(8,128)(2,1)S(1)}, u32[]{:S(2)}, u32[]{:S(2)}) async-start(bf16[2,256,512]{1,2,0:T(8,128)(2,1)} %copy.24), calls=%async_computation | async-start | bytes 1048576 | tf_op jit(solution)/shard_map/all_to_all | solution.py:92
  34.0 7.5 %all-to-all-done = bf16[2,256,512]{1,2,0:T(8,128)(2,1)S(1)} async-done(((bf16[2,256,512]{1,2,0:T(8,128)(2,1)}), bf16[2,256,512]{1,2,0:T(8,128)(2,1)S(1)}, u32[]{:S(2)}, u32[]{:S(2)}) %all-to-all-start) | async-done | bytes 524320 | tf_op jit(solution)/shard_map/all_to_all | solution.py:92
  41.5 3.6 %fusion.15 = (f32[256]{0:T(256)S(1)}, bf16[256,2048]{1,0:T(8,128)(2,1)S(1)}) fusion(bf16[256,1024]{0,1:T(8,128)(2,1)S(1)} %bitcast.82, bf16[1024,2048]{1,0:T(8,128)(2,1)} %param.16, bf16[256,2048]{1,0:T(8,128)(2,1)S(1)} %copy-done.5), kind=kOutput, calls=%fused_computation.22 | convolution fusion | flops 1076887296 | bytes 6816768 | tf_op jit(solution)/shard_map/dot_general | solution.py:93
  45.5 1.3 broadcast_in_dim.49
  46.7 2.2 reshape.145
  49.0 7.2 %scatter_custom_fusion = bf16[1024,2048]{1,0:T(8,128)(2,1)} fusion(s32[512]{0:T(512)S(1)} %bitcast.83, bf16[512,2048]{1,0:T(8,128)(2,1)} %reshape.145, bf16[]{:T(256)} %constant.60.clone.1), kind=kCustom, calls=%fused_computation.26 | custom fusion | bytes 4194816 | tf_op jit(solution)/shard_map/scatter | solution.py:115
  56.2 101.2 %all_to_all.29 = bf16[32,32,2048]{2,1,0:T(8,128)(2,1)S(1)} all-to-all(bf16[32,32,2048]{2,1,0:T(8,128)(2,1)} %bitcast.77), channel_id=1, replica_groups=mesh['sp'=16,'tp'=2] {'sp','tp'}, dimensions={0} | all-to-all | bytes 8388608 | tf_op jit(solution)/shard_map/all_to_all | solution.py:119
  157.4 4.5 %fusion.5 = f32[1024,1024]{1,0:T(8,128)S(1)} fusion(bf16[1024,2048]{1,0:T(8,128)(2,1)S(1)} %bitcast.79, bf16[1,2048,1024]{2,1,0:T(8,128)(2,1)S(1)} %copy-done.2), kind=kOutput, calls=%fused_computation.10 | convolution fusion | flops 4294967296 | bytes 12582912 | tf_op jit(solution)/shard_map/dot_general | solution.py:31
  162.0 5.4 %multiply_convert_fusion = bf16[1024,1024]{1,0:T(8,128)(2,1)S(1)} fusion(f32[1024,1024]{1,0:T(8,128)S(1)} %fusion.5, bf16[1024,2048]{1,0:T(8,128)(2,1)S(1)} %bitcast.80, bf16[1,2048,1024]{2,1,0:T(8,128)(2,1)S(1)} %copy-done.3), kind=kOutput, calls=%fused_computation.15 | convolution fusion | flops 4301258752 | bytes 14680064 | tf_op jit(solution)/shard_map/dot_general | solution.py:30
  167.4 6.1 %fusion.9 = bf16[1024,2048]{1,0:T(8,128)(2,1)} fusion(bf16[1024,1024]{1,0:T(8,128)(2,1)S(1)} %multiply_convert_fusion, bf16[1,1024,2048]{2,1,0:T(8,128)(2,1)S(1)} %copy-done.4), kind=kOutput, calls=%fused_computation.16 | convolution fusion | flops 4297064448 | bytes 10485760 | tf_op jit(solution)/shard_map/dot_general | solution.py:33
  173.5 4.0 %all-to-all-start.2 = ((bf16[32,32,2048]{2,1,0:T(8,128)(2,1)}), bf16[32,32,2048]{2,1,0:T(8,128)(2,1)}, u32[]{:S(2)}, u32[]{:S(2)}) async-start(bf16[32,32,2048]{2,1,0:T(8,128)(2,1)} %bitcast.78), calls=%async_computation.2 | async-start | bytes 8388608 | tf_op jit(solution)/shard_map/all_to_all | solution.py:124
  177.7 93.3 %all-to-all-done.2 = bf16[32,32,2048]{2,1,0:T(8,128)(2,1)} async-done(((bf16[32,32,2048]{2,1,0:T(8,128)(2,1)}), bf16[32,32,2048]{2,1,0:T(8,128)(2,1)}, u32[]{:S(2)}, u32[]{:S(2)}) %all-to-all-start.2) | async-done | bytes 4194336 | tf_op jit(solution)/shard_map/all_to_all | solution.py:124
  271.0 7.1 %gather_fusion = bf16[512,2048]{1,0:T(8,128)(2,1)S(1)} fusion(bf16[1024,2048]{1,0:T(8,128)(2,1)} %bitcast.18, s32[1024]{0:T(1024)S(1)} %pad_clamp_fusion), kind=kCustom, calls=%fused_computation | custom fusion | bytes 4196352 | tf_op jit(solution)/shard_map/gather | solution.py:126
  278.1 4.0 %reshape.132 = f32[256,2,2048]{2,1,0:T(2,128)} reshape(bf16[512,2048]{1,0:T(8,128)(2,1)S(1)} %gather_fusion) | data formatting | bytes 6291456 | tf_op jit(solution)/shard_map/convert_element_type | solution.py:126
  282.1 8.9 %multiply_reduce_fusion = f32[256,2048]{1,0:T(8,128)S(1)} fusion(f32[256,2,2048]{2,1,0:T(2,128)} %reshape.132, f32[256,2]{1,0:T(8,128)S(1)} %copy.29), kind=kLoop, calls=%fused_computation.14 | loop fusion | flops 1572864 | bytes 6293504 | tf_op jit(solution)/shard_map/reduce_sum | solution.py:127
  291.0 1.3 fusion.18
  (48 shorter events, 9.9 us)
Async XLA Ops:
  0.8 16.7 %collective-permute-start.2 = (s32[128]{0:T(128)S(1)}, s32[128]{0:T(128)S(1)}, u32[]{:S(2)}, u32[]{:S(2)}) collective-permute-start(s32[128]{0:T(128)S(1)} %get-tuple-element.21), channel_id=1, source_target_pairs={{0,2},{2,4},{4,6},{6,8},{8,10},{10,12},{12,14},{14,16},{16,18},{18... | collective-permute-start | bytes 1544 | tf_op jit(solution)/shard_map/ppermute | solution.py:18
  3.2 14.3 %collective-permute-start.3 = (s32[128]{0:T(128)S(1)}, s32[128]{0:T(128)S(1)}, u32[]{:S(2)}, u32[]{:S(2)}) collective-permute-start(s32[128]{0:T(128)S(1)} %get-tuple-element.22), channel_id=1, source_target_pairs={{2,0},{4,2},{6,4},{8,6},{10,8},{12,10},{14,12},{16,14},{18,16},{20... | collective-permute-start | bytes 1544 | tf_op jit(solution)/shard_map/ppermute | solution.py:20
  5.6 14.1 %collective-permute-start = (bf16[128,2,128]{0,2,1:T(8,128)(2,1)S(1)}, bf16[128,2,128]{0,2,1:T(8,128)(2,1)S(1)}, u32[]{:S(2)}, u32[]{:S(2)}) collective-permute-start(bf16[128,2,128]{0,2,1:T(8,128)(2,1)S(1)} %get-tuple-element.19), channel_id=1, source_target_pairs={{0,2},{2,4},{4,6},{6,8},{8,10},{10,12},{12,14},{14,16},{16,18},{18... | collective-permute-start | bytes 196616 | tf_op jit(solution)/shard_map/ppermute | solution.py:18
  10.8 8.9 %collective-permute-start.1 = (bf16[128,2,128]{0,2,1:T(8,128)(2,1)S(1)}, bf16[128,2,128]{0,2,1:T(8,128)(2,1)S(1)}, u32[]{:S(2)}, u32[]{:S(2)}) collective-permute-start(bf16[128,2,128]{0,2,1:T(8,128)(2,1)S(1)} %get-tuple-element.20), channel_id=1, source_target_pairs={{2,0},{4,2},{6,4},{8,6},{10,8},{12,10},{14,12},{16,14},{18,16},{20... | collective-permute-start | bytes 196616 | tf_op jit(solution)/shard_map/ppermute | solution.py:20
  25.1 16.4 %copy-start.5 = (bf16[256,2048]{1,0:T(8,128)(2,1)S(1)}, bf16[256,2048]{1,0:T(8,128)(2,1)}, u32[]{:S(2)}) copy-start(bf16[256,2048]{1,0:T(8,128)(2,1)} %param.17) | copy-start | bytes 3145732
  30.0 11.5 %all-to-all-start = ((bf16[2,256,512]{1,2,0:T(8,128)(2,1)}), bf16[2,256,512]{1,2,0:T(8,128)(2,1)S(1)}, u32[]{:S(2)}, u32[]{:S(2)}) async-start(bf16[2,256,512]{1,2,0:T(8,128)(2,1)} %copy.24), calls=%async_computation | async-start | bytes 1048576 | tf_op jit(solution)/shard_map/all_to_all | solution.py:92
  34.0 11.1 %copy-start = (f32[2048]{0:T(1024)S(1)}, f32[2048]{0:T(1024)}, u32[]{:S(2)}) copy-start(f32[2048]{0:T(1024)} %param.18) | copy-start | bytes 24580
  56.2 101.2 %copy-start.2 = (bf16[1,2048,1024]{2,1,0:T(8,128)(2,1)S(1)}, bf16[1,2048,1024]{2,1,0:T(8,128)(2,1)}, u32[]{:S(2)}) copy-start(bf16[1,2048,1024]{2,1,0:T(8,128)(2,1)} %param.20) | copy-start | bytes 12582916
  157.4 4.5 %copy-start.3 = (bf16[1,2048,1024]{2,1,0:T(8,128)(2,1)S(1)}, bf16[1,2048,1024]{2,1,0:T(8,128)(2,1)}, u32[]{:S(2)}) copy-start(bf16[1,2048,1024]{2,1,0:T(8,128)(2,1)} %param.19) | copy-start | bytes 12582916
  162.0 5.4 %copy-start.4 = (bf16[1,1024,2048]{2,1,0:T(8,128)(2,1)S(1)}, bf16[1,1024,2048]{2,1,0:T(8,128)(2,1)}, u32[]{:S(2)}) copy-start(bf16[1,1024,2048]{2,1,0:T(8,128)(2,1)} %param.21) | copy-start | bytes 12582916
  173.5 4.0 %copy-start.1 = (f32[256,2]{0,1:T(2,128)S(1)}, f32[256,2]{0,1:T(2,128)}, u32[]{:S(2)}) copy-start(f32[256,2]{0,1:T(2,128)} %param.23) | copy-start | bytes 6148
  173.5 97.5 %all-to-all-start.2 = ((bf16[32,32,2048]{2,1,0:T(8,128)(2,1)}), bf16[32,32,2048]{2,1,0:T(8,128)(2,1)}, u32[]{:S(2)}, u32[]{:S(2)}) async-start(bf16[32,32,2048]{2,1,0:T(8,128)(2,1)} %bitcast.78), calls=%async_computation.2 | async-start | bytes 8388608 | tf_op jit(solution)/shard_map/all_to_all | solution.py:124
where the time goes:
time: 293 us; the launch traced here: 292 us
  waiting for transfers between devices  101 us (34%)
  blocking collectives  101 us (34%)
  local copies, waits for them, and re-layouts  28.5 us (10%)
  matrix products  25.7 us (9%)
  other arithmetic  18 us (6%)
  starting transfers between devices  17.8 us (6%)
    all_to_all x1, blocking collectives, shards(): lax.all_to_all(sent, ('sp', 'tp'), split_axis=0, concat_axis=0, tiled=True)  101 us
    all_to_all x1, waiting for transfers between devices, shards(): lax.all_to_all(finished, ('sp', 'tp'), split_axis=0, concat_axis=0, tiled...  93.3 us
    reduce_sum x1, other arithmetic, shards(): mixture = jnp.sum(picked * route_weight[..., None], axis=1)  8.89 us
    ppermute x2, starting transfers between devices, with_halo(): lax.ppermute(tail, axis, [(i, (i + 1) % count) for i in range(ends)])  7.54 us
    all_to_all x1, waiting for transfers between devices, shards(): lax.all_to_all(attended, 'tp', split_axis=0, concat_axis=1, tiled=True)  7.47 us
    scatter x1, local copies, waits for them, and re-layouts, shards(): jnp.zeros((expert_count * capacity, width), jnp.bfloat16).at[slot_index]  7.21 us
    gather x1, local copies, waits for them, and re-layouts, shards(): returned[slot_index].astype(jnp.float32).reshape(local_rows, topk, width)  7.13 us
    dot_general x1, matrix products, expert_rows(): jnp.dot(expert_hidden, down_w, preferred_element_type=jnp.float32)  6.15 us
  transfers between devices with their start and end apart: 6, of which 2 were waited for; matrix products, arithmetic and copies ran while one was open for 3% of the time, Pallas kernels for 0%

commit v1 on v0

--- a/solution.py
+++ b/solution.py
@@ -1,27 +1,394 @@
+import functools
+
 import jax
 import jax.numpy as jnp
 from jax import lax
+from jax.experimental import pallas as pl
+from jax.experimental.pallas import tpu as pltpu
 from jax.sharding import PartitionSpec as P
 
 HD = 64
 WIN = 128
-
-
-def with_halo(cells, sides, width):
-    for axis, dim in sides:
-        count = lax.axis_size(axis)
-        ends = count - 1
-        head = lax.slice_in_dim(cells, 0, width, axis=dim)
-        tail = lax.slice_in_dim(cells, cells.shape[dim] - width, cells.shape[dim], axis=dim)
-        cells = jnp.concatenate(
-            [
-                lax.ppermute(tail, axis, [(i, (i + 1) % count) for i in range(ends)]),
-                cells,
-                lax.ppermute(head, axis, [((i + 1) % count, i) for i in range(ends)]),
-            ],
-            axis=dim,
-        )
-    return cells
+PLANES = 4
+CUTS = 2
+MESH = pl.DeviceIdType.MESH
+
+
+def with_halo(cells, axis, width):
+    count = lax.axis_size(axis)
+    ends = count - 1
+    return jnp.concatenate(
+        [
+            lax.ppermute(cells[-width:], axis, [(i, (i + 1) % count) for i in range(ends)]),
+            cells,
+            lax.ppermute(cells[:width], axis, [((i + 1) % count, i) for i in range(ends)]),
+        ],
+        axis=0,
+    )
+
+
+def place(stride, tps):
+    sp = lax.axis_index("sp")
+    tp = lax.axis_index("tp")
+    return lax.div(sp, stride), lax.rem(sp, stride), tp, lax.rem(sp, stride) * tps + tp
+
+
+def greet(z, r, tp, p, planes, stride, tps):
+    peers = stride * tps
+    barrier = pltpu.get_barrier_semaphore()
+    for k in range(1, peers):
+        pd = lax.rem(p + k, peers)
+        pl.semaphore_signal(
+            barrier,
+            inc=1,
+            device_id=(z * stride + lax.div(pd, tps), lax.rem(pd, tps)),
+            device_id_type=MESH,
+        )
+
+    @pl.when(z > 0)
+    def _():
+        pl.semaphore_signal(
+            barrier, inc=1, device_id=((z - 1) * stride + r, tp), device_id_type=MESH
+        )
+
+    @pl.when(z < planes - 1)
+    def _():
+        pl.semaphore_signal(
+            barrier, inc=1, device_id=((z + 1) * stride + r, tp), device_id_type=MESH
+        )
+
+    beside = (z > 0).astype(jnp.int32) + (z < planes - 1).astype(jnp.int32)
+    pl.semaphore_wait(barrier, peers - 1 + beside)
+
+
+def slot_hits(tab, z, slots, rows):
+    ids = lax.broadcasted_iota(jnp.int32, (slots, rows), 0) + z * slots
+    ids = ids.astype(jnp.float32)
+    return ids == tab[0:1, :], ids == tab[1:2, :]
+
+
+def dispatch_kernel(
+    planes, stride, tps, cap,
+    x_ref, tab_ref, out_ref,
+    toks, stage, zsend, zrecv, psend, precv, lsem,
+):
+    z, r, tp, p = place(stride, tps)
+    peers = stride * tps
+    rows, width = x_ref.shape
+    cols = width // CUTS
+    slots = peers * cap
+    greet(z, r, tp, p, planes, stride, tps)
+
+    def span(h):
+        return pl.ds(pl.multiple_of(h * cols, cols), cols)
+
+    def hop(zs, h, side):
+        return pltpu.make_async_remote_copy(
+            src_ref=toks.at[zs, :, span(h)],
+            dst_ref=toks.at[zs, :, span(h)],
+            send_sem=zsend.at[side, zs, h],
+            recv_sem=zrecv.at[zs, h],
+            device_id=((z + 1 - 2 * side) * stride + r, tp),
+            device_id_type=MESH,
+        )
+
+    def own_hop(h, side):
+        return pltpu.make_async_remote_copy(
+            src_ref=x_ref.at[:, span(h)],
+            dst_ref=toks.at[z, :, span(h)],
+            send_sem=zsend.at[side, z, h],
+            recv_sem=zrecv.at[z, h],
+            device_id=((z + 1 - 2 * side) * stride + r, tp),
+            device_id_type=MESH,
+        )
+
+    def plane_copy(zs, h, dest, at):
+        return pltpu.make_async_remote_copy(
+            src_ref=stage.at[zs, pl.ds(pl.multiple_of(dest * cap, cap), cap), span(h)],
+            dst_ref=out_ref.at[zs, at, :, span(h)],
+            send_sem=psend.at[zs, h, dest],
+            recv_sem=precv.at[zs, h, at],
+            device_id=(z * stride + lax.div(dest, tps), lax.rem(dest, tps)),
+            device_id_type=MESH,
+        )
+
+    def local_copy(zs, h):
+        return pltpu.make_async_copy(
+            stage.at[zs, pl.ds(pl.multiple_of(p * cap, cap), cap), span(h)],
+            out_ref.at[zs, p, :, span(h)],
+            lsem.at[zs, h],
+        )
+
+    def pack(block, zs, h):
+        tab = tab_ref[lax.rem(z - zs + planes, planes)]
+        first, second = slot_hits(tab, z, slots, rows)
+        pick = jnp.where(first | second, 1.0, 0.0).astype(jnp.bfloat16)
+        stage[zs, :, span(h)] = jnp.dot(
+            pick, block, preferred_element_type=jnp.float32
+        ).astype(jnp.bfloat16)
+        for k in range(1, peers):
+            plane_copy(zs, h, lax.rem(p + k, peers), p).start()
+        local_copy(zs, h).start()
+
+    for h in range(CUTS):
+
+        @pl.when(z < planes - 1)
+        def _():
+            own_hop(h, 0).start()
+
+        @pl.when(z > 0)
+        def _():
+            own_hop(h, 1).start()
+
+    @pl.loop(0, CUTS)
+    def _(h):
+        pack(x_ref[:, span(h)], z, h)
+
+    @pl.loop(0, 2 * CUTS * (planes - 1))
+    def _(e):
+        dist = lax.div(e, 2 * CUTS) + 1
+        h = lax.rem(lax.div(e, 2), CUTS)
+        side = lax.rem(e, 2)
+        zs = z - dist + 2 * dist * side
+
+        @pl.when((zs >= 0) & (zs < planes))
+        def _():
+            hop(zs, h, side).wait_recv()
+            onward = z + 1 - 2 * side
+
+            @pl.when((onward >= 0) & (onward < planes))
+            def _():
+                hop(zs, h, side).start()
+
+            pack(toks[zs, :, span(h)], zs, h)
+
+    @pl.loop(0, planes * CUTS)
+    def _(e):
+        zs = lax.div(e, CUTS)
+        h = lax.rem(e, CUTS)
+
+        @pl.when((zs <= z) & (z < planes - 1))
+        def _():
+            hop(zs, h, 0).wait_send()
+
+        @pl.when((zs >= z) & (z > 0))
+        def _():
+            hop(zs, h, 1).wait_send()
+
+        local_copy(zs, h).wait()
+        for k in range(1, peers):
+            other = lax.rem(p + k, peers)
+            plane_copy(zs, h, other, p).wait_send()
+            plane_copy(zs, h, other, other).wait_recv()
+
+
+def return_kernel(
+    planes, stride, tps, cap,
+    y_ref, tab_ref, mid_ref, out_ref,
+    held, part, from_low, from_high, zsend, lowrecv, highrecv, psend, precv, lsem, total,
+):
+    z, r, tp, p = place(stride, tps)
+    peers = stride * tps
+    rows, width = mid_ref.shape
+    cols = width // CUTS
+    slots = peers * cap
+    greet(z, r, tp, p, planes, stride, tps)
+
+    def span(h):
+        return pl.ds(pl.multiple_of(h * cols, cols), cols)
+
+    def plane_copy(zs, h, dest, at):
+        return pltpu.make_async_remote_copy(
+            src_ref=y_ref.at[zs, dest, :, span(h)],
+            dst_ref=held.at[zs, pl.ds(pl.multiple_of(at * cap, cap), cap), span(h)],
+            send_sem=psend.at[zs, h, dest],
+            recv_sem=precv.at[zs, h, at],
+            device_id=(z * stride + lax.div(dest, tps), lax.rem(dest, tps)),
+            device_id_type=MESH,
+        )
+
+    def local_copy(zs, h):
+        return pltpu.make_async_copy(
+            y_ref.at[zs, p, :, span(h)],
+            held.at[zs, pl.ds(pl.multiple_of(p * cap, cap), cap), span(h)],
+            lsem.at[zs, h],
+        )
+
+    def send_out(zs, h):
+        for k in range(1, peers):
+            plane_copy(zs, h, lax.rem(p + k, peers), p).start()
+        local_copy(zs, h).start()
+
+    def up(zs, h):
+        return pltpu.make_async_remote_copy(
+            src_ref=part.at[zs, :, span(h)],
+            dst_ref=from_low.at[zs, :, span(h)],
+            send_sem=zsend.at[zs, h],
+            recv_sem=lowrecv.at[zs, h],
+            device_id=((z + 1) * stride + r, tp),
+            device_id_type=MESH,
+        )
+
+    def down(zs, h):
+        return pltpu.make_async_remote_copy(
+            src_ref=part.at[zs, :, span(h)],
+            dst_ref=from_high.at[zs, :, span(h)],
+            send_sem=zsend.at[zs, h],
+            recv_sem=highrecv.at[zs, h],
+            device_id=((z - 1) * stride + r, tp),
+            device_id_type=MESH,
+        )
+
+    def combined(zs, h):
+        local_copy(zs, h).wait()
+        for k in range(1, peers):
+            plane_copy(zs, h, p, lax.rem(p + k, peers)).wait_recv()
+        tab = tab_ref[lax.rem(z - zs + planes, planes)]
+        first, second = slot_hits(tab, z, slots, rows)
+        mix = jnp.where(first, tab[2:3, :], 0.0) + jnp.where(second, tab[3:4, :], 0.0)
+        return jnp.dot(
+            mix.T.astype(jnp.bfloat16), held[zs, :, span(h)], preferred_element_type=jnp.float32
+        )
+
+    events = 2 * CUTS * (planes - 1)
+
+    def event(e):
+        dist = planes - 1 - lax.div(e, 2 * CUTS)
+        h = lax.rem(lax.div(e, 2), CUTS)
+        side = lax.rem(e, 2)
+        zs = z + dist - 2 * dist * side
+        return zs, h, side
+
+    @pl.loop(0, events)
+    def _(e):
+        zs, h, side = event(e)
+
+        @pl.when((zs >= 0) & (zs < planes))
+        def _():
+            send_out(zs, h)
+
+    @pl.loop(0, CUTS)
+    def _(h):
+        send_out(z, h)
+
+    @pl.loop(0, events)
+    def _(e):
+        zs, h, side = event(e)
+
+        @pl.when((zs >= 0) & (zs < planes))
+        def _():
+            mine = combined(zs, h)
+            part[zs, :, span(h)] = mine.astype(jnp.bfloat16)
+
+            @pl.when((side == 0) & (z > 0))
+            def _():
+                up(zs, h).wait_recv()
+                part[zs, :, span(h)] = (
+                    part[zs, :, span(h)].astype(jnp.float32)
+                    + from_low[zs, :, span(h)].astype(jnp.float32)
+                ).astype(jnp.bfloat16)
+
+            @pl.when((side == 1) & (z < planes - 1))
+            def _():
+                down(zs, h).wait_recv()
+                part[zs, :, span(h)] = (
+                    part[zs, :, span(h)].astype(jnp.float32)
+                    + from_high[zs, :, span(h)].astype(jnp.float32)
+                ).astype(jnp.bfloat16)
+
+            @pl.when(side == 0)
+            def _():
+                up(zs, h).start()
+
+            @pl.when(side == 1)
+            def _():
+                down(zs, h).start()
+
+    @pl.loop(0, CUTS)
+    def _(h):
+        total[:, span(h)] = mid_ref[:, span(h)].astype(jnp.float32) + combined(z, h)
+
+        @pl.when(z > 0)
+        def _():
+            up(z, h).wait_recv()
+            total[:, span(h)] += from_low[z, :, span(h)].astype(jnp.float32)
+
+        @pl.when(z < planes - 1)
+        def _():
+            down(z, h).wait_recv()
+            total[:, span(h)] += from_high[z, :, span(h)].astype(jnp.float32)
+
+        out_ref[:, span(h)] = total[:, span(h)].astype(jnp.bfloat16)
+
+    @pl.loop(0, planes * CUTS)
+    def _(e):
+        zs = lax.div(e, CUTS)
+        h = lax.rem(e, CUTS)
+
+        @pl.when(zs > z)
+        def _():
+            up(zs, h).wait_send()
+
+        @pl.when(zs < z)
+        def _():
+            down(zs, h).wait_send()
+
+        for k in range(1, peers):
+            plane_copy(zs, h, lax.rem(p + k, peers), p).wait_send()
+
+
+def routed_by_plane(normed, mid, tables, cap, weights):
+    planes = tables.shape[0]
+    rows, width = normed.shape
+    tps = lax.axis_size("tp")
+    stride = lax.axis_size("sp") // planes
+    peers = stride * tps
+    dma = pltpu.SemaphoreType.DMA
+    vmem = pl.BlockSpec(memory_space=pltpu.VMEM)
+    anywhere = pl.BlockSpec(memory_space=pl.ANY)
+    arrived = pl.pallas_call(
+        functools.partial(dispatch_kernel, planes, stride, tps, cap),
+        out_shape=jax.ShapeDtypeStruct((planes, peers, cap, width), jnp.bfloat16),
+        in_specs=[vmem, vmem],
+        out_specs=anywhere,
+        scratch_shapes=[
+            pltpu.VMEM((planes, rows, width), jnp.bfloat16),
+            pltpu.VMEM((planes, peers * cap, width), jnp.bfloat16),
+            dma((2, planes, CUTS)),
+            dma((planes, CUTS)),
+            dma((planes, CUTS, peers)),
+            dma((planes, CUTS, peers)),
+            dma((planes, CUTS)),
+        ],
+        compiler_params=pltpu.CompilerParams(
+            collective_id=0, has_side_effects=True, vmem_limit_bytes=32 * 1024 * 1024
+        ),
+        name="dispatch",
+    )(normed, tables)
+    finished = expert_rows(arrived, *weights)
+    return pl.pallas_call(
+        functools.partial(return_kernel, planes, stride, tps, cap),
+        out_shape=jax.ShapeDtypeStruct((rows, width), jnp.bfloat16),
+        in_specs=[anywhere, vmem, vmem],
+        out_specs=vmem,
+        scratch_shapes=[
+            pltpu.VMEM((planes, peers * cap, width), jnp.bfloat16),
+            pltpu.VMEM((planes, rows, width), jnp.bfloat16),
+            pltpu.VMEM((planes, rows, width), jnp.bfloat16),
+            pltpu.VMEM((planes, rows, width), jnp.bfloat16),
+            dma((planes, CUTS)),
+            dma((planes, CUTS)),
+            dma((planes, CUTS)),
+            dma((planes, CUTS, peers)),
+            dma((planes, CUTS, peers)),
+            dma((planes, CUTS)),
+            pltpu.VMEM((rows, width), jnp.float32),
+        ],
+        compiler_params=pltpu.CompilerParams(
+            collective_id=1, has_side_effects=True, vmem_limit_bytes=40 * 1024 * 1024
+        ),
+        name="combine",
+    )(finished, tables, mid)
 
 
 def expert_rows(arrived, gate_w, up_w, down_w):
@@ -53,10 +420,15 @@
     kv_here = keys_values.shape[1]
     group = heads_here // kv_here
     head_dim = keys_values.shape[2] // 2
-    kv_ext, docs_ext = (
-        with_halo(keys_values, (("sp", 0),), WIN),
-        with_halo(doc_ids, (("sp", 0),), WIN),
-    )
+    docs_wide = jnp.broadcast_to(
+        doc_ids.astype(jnp.bfloat16)[:, None], (tok_here, keys_values.shape[2])
+    )
+    slab = jnp.concatenate([keys_values.reshape(tok_here, -1), docs_wide], axis=1)
+    slab = with_halo(slab, "sp", WIN)
+    kv_ext = slab[:, : kv_here * keys_values.shape[2]].reshape(
+        -1, kv_here, keys_values.shape[2]
+    )
+    docs_ext = slab[:, kv_here * keys_values.shape[2]].astype(jnp.int32)
     offset = lax.axis_index("sp") * tok_here
     seq_total = lax.axis_size("sp") * tok_here
     span_rows = min(512, tok_here)
@@ -89,7 +461,18 @@
     attended = lax.map(one_span, jnp.arange(tok_here // span_rows, dtype=jnp.int32)).reshape(
         tok_here, -1
     )
-    gathered = lax.all_to_all(attended, "tp", split_axis=0, concat_axis=1, tiled=True)
+    if lax.axis_size("tp") == 2:
+        tp = lax.axis_index("tp")
+        half = tok_here // 2
+        mine = lax.dynamic_slice_in_dim(attended, tp * half, half, 0)
+        other = lax.ppermute(
+            lax.dynamic_slice_in_dim(attended, (1 - tp) * half, half, 0), "tp", [(0, 1), (1, 0)]
+        )
+        gathered = jnp.concatenate(
+            [jnp.where(tp == 0, mine, other), jnp.where(tp == 0, other, mine)], axis=1
+        )
+    else:
+        gathered = lax.all_to_all(attended, "tp", split_axis=0, concat_axis=1, tiled=True)
     projected = jnp.dot(gathered, out_weight, preferred_element_type=jnp.float32)
     mid_wide = (hidden_in.astype(jnp.float32) + projected).astype(jnp.bfloat16).astype(jnp.float32)
     normed = (
@@ -110,6 +493,32 @@
     )
     slot_rank = (jnp.cumsum(one_hot, axis=0) * one_hot).sum(-1) - 1
     slot_index = flat_routes * capacity + slot_rank
+    if capacity % 16 == 0 and sp_count % PLANES == 0 and topk == 2:
+        tab = jnp.concatenate(
+            [
+                slot_index.reshape(local_rows, topk).astype(jnp.float32).T,
+                route_weight.T,
+                jnp.zeros((4, local_rows), jnp.float32),
+            ],
+            axis=0,
+        )
+        stride = sp_count // PLANES
+        tables = jnp.stack(
+            [tab]
+            + [
+                lax.ppermute(
+                    tab, "sp", [(i, (i + d * stride) % sp_count) for i in range(sp_count)]
+                )
+                for d in range(1, PLANES)
+            ]
+        )
+        return routed_by_plane(
+            normed,
+            mid_wide.astype(jnp.bfloat16),
+            tables,
+            capacity,
+            (expert_gate[0], expert_up[0], expert_down[0]),
+        )
     repeated = jnp.repeat(normed, topk, axis=0)
     buffer_rows = (
         jnp.zeros((expert_count * capacity, width), jnp.bfloat16).at[slot_index].set(repeated)

time: 293 us -> 214 us (0.73)
  Pallas kernels: 0 us -> 158 us
  blocking collectives: 101 us -> 0 us
  waiting for transfers between devices: 101 us -> 2.31 us
  local copies, waits for them, and re-layouts: 28.5 us -> 5.81 us
  other arithmetic: 18 us -> 7.47 us
    pallas_call x0 -> x2, Pallas kernels: none -> 158 us  [the longest x1 79.8 us: routed_by_plane(): pl.pallas_call(functools.partial(return_kernel, planes, stride, tps, cap)...]
    all_to_all x1 -> x0, blocking collectives: 101 us -> none  [shards(): lax.all_to_all(sent, ('sp', 'tp'), split_axis=0, concat_axis=0, tiled=True)]
    all_to_all x2 -> x0, waiting for transfers between devices: 101 us -> none  [the longest x1 93.3 us: shards(): lax.all_to_all(finished, ('sp', 'tp'), split_axis=0, concat_axis=0, tiled...]
    reduce_sum x1 -> x0, other arithmetic: 8.89 us -> none  [shards(): mixture = jnp.sum(picked * route_weight[..., None], axis=1)]
    all_to_all x2 -> x0, starting transfers between devices: 7.7 us -> none  [the longest x1 4.03 us: shards(): lax.all_to_all(finished, ('sp', 'tp'), split_axis=0, concat_axis=0, tiled...]
    scatter x1 -> x0, local copies, waits for them, and re-layouts: 7.21 us -> none  [shards(): jnp.zeros((expert_count * capacity, width), jnp.bfloat16).at[slot_index]]
    gather x1 -> x0, local copies, waits for them, and re-layouts: 7.13 us -> none  [shards(): returned[slot_index].astype(jnp.float32).reshape(local_rows, topk, width)]
    ppermute x4 -> x6, starting transfers between devices: 10.1 us -> 15 us  [the longest x3 8.93 us: shards(): lax.ppermute(tab, 'sp', [(i, (i + d * stride) % sp_count) for i in range(...]
where the time goes in v1:
time: 214 us; the launch traced here: 213 us
  Pallas kernels  158 us (74%)
  matrix products  24.2 us (11%)
  starting transfers between devices  15 us (7%)
  other arithmetic  7.47 us (3%)
  local copies, waits for them, and re-layouts  5.81 us (3%)
  waiting for transfers between devices  2.31 us (1%)
    pallas_call x1, Pallas kernels, routed_by_plane(): pl.pallas_call(functools.partial(return_kernel, planes, stride, tps, cap)...  79.8 us
    pallas_call x1, Pallas kernels, routed_by_plane(): pl.pallas_call(functools.partial(dispatch_kernel, planes, stride, tps, ca...  78.5 us
    ppermute x3, starting transfers between devices, shards(): lax.ppermute(tab, 'sp', [(i, (i + d * stride) % sp_count) for i in range(...  8.93 us
    dot_general x1, matrix products, expert_rows(): gate = jnp.dot(flat_rows, gate_w, preferred_element_type=jnp.float32)  5.31 us
    dot_general x1, matrix products, expert_rows(): jnp.dot(expert_hidden, down_w, preferred_element_type=jnp.float32)  4.71 us
    dot_general x1, matrix products, expert_rows(): upper = jnp.dot(flat_rows, up_w, preferred_element_type=jnp.float32)  4.48 us
  transfers between devices with their start and end apart: 6, of which 2 were waited for; matrix products, arithmetic and copies ran while one was open for 3% of the time, Pallas kernels for 0%

profile of v1, /device:TPU:0, one launch (start us, length us, event | category | flops | bytes accessed | tf_op | source)
XLA Modules:
  0.0 213.5 jit_solution(7846715182414241605)
XLA Ops:
  0.0 1.1 copy.26
  1.9 2.4 %collective-permute-start = (bf16[128,384]{0,1:T(8,128)(2,1)S(1)}, bf16[128,384]{0,1:T(8,128)(2,1)S(1)}, u32[]{:S(2)}, u32[]{:S(2)}) collective-permute-start(bf16[128,384]{0,1:T(8,128)(2,1)S(1)} %get-tuple-element.21), channel_id=1, source_target_pairs={{0,2},{2,4},{4,6},{6,8},{8,10},{10,12},{12,14},{14,16},{16,18},{18... | collective-permute-start | bytes 294920 | tf_op jit(solution)/shard_map/ppermute | solution.py:22
  4.3 1.3 collective-permute-start.1
  5.6 0.8 copy.19
  6.7 1.3 copy.17
  8.0 0.7 max.22
  8.7 1.2 reduce-window.6
  10.5 0.7 convert_bitcast_fusion
  11.4 0.9 fusion.19
  12.3 2.1 fusion
  14.5 3.1 %fusion.1 = f32[2,4,512]{2,1,0:T(4,128)S(1)} fusion(f32[2,768,512,4]{2,1,3,0:T(8,128)S(1)} %get-tuple-element.36, f32[2,4,512]{2,1,0:T(4,128)S(1)} %broadcast_maximum_fusion, pred[512,768]{0,1:T(8,128)(4,1)S(1)} %fusion.19), kind=kLoop, calls=%fused_computation.4 | loop fusion | flops 15724544 | bytes 13008896 | tf_op jit(solution)/shard_map/while/body/eval_jaxpr/reduce_sum | solution.py:454
  17.7 4.0 %fusion.20 = bf16[2,64,4,512]{3,1,2,0:T(8,128)(2,1)S(1)} fusion(f32[2,768,512,4]{2,1,3,0:T(8,128)S(1)} %get-tuple-element.36, f32[2,4,512]{2,1,0:T(4,128)S(1)} %exponential_add_fusion, f32[2,4,512]{2,1,0:T(4,128)S(1)} %broadcast_maximum_fusion, pred[512,768]{0,1:T(8,128)(4,1)S(1)} %fusion.19, bf16[768,2,128]{0,2,1:T(8,128)(2,1)S(1)} %bitcast.82), kind=kOutput, calls=%fused_computation.24 | convolution fusion | flops 421789696 | bytes 13729792 | tf_op jit(solution)/shard_map/while/body/eval_jaxpr/hgqk,khd->qhgd/dot_general | solution.py:456
  21.7 2.4 %collective-permute-start.2 = (bf16[256,512]{0,1:T(8,128)(2,1)S(1)}, bf16[256,512]{0,1:T(8,128)(2,1)S(1)}, u32[]{:S(2)}, u32[]{:S(2)}) collective-permute-start(bf16[256,512]{0,1:T(8,128)(2,1)S(1)} %constant_dynamic-slice_fusion), channel_id=1, source_target_pairs={{0,1},{1,0},{2,3},{3,2},{4,5},{5,4},{6,7},{7,6},{8,9},{9,8},{10,11... | collective-permute-start | bytes 786440 | tf_op jit(solution)/shard_map/ppermute | solution.py:468
  24.2 5.0 %collective-permute-start.3 = (f32[8,256]{1,0:T(8,128)S(1)}, f32[8,256]{1,0:T(8,128)S(1)}, u32[]{:S(2)}, u32[]{:S(2)}) collective-permute-start(f32[8,256]{1,0:T(8,128)S(1)} %get-tuple-element.32), channel_id=1, source_target_pairs={{0,8},{2,10},{4,12},{6,14},{8,16},{10,18},{12,20},{14,22},{16,24},... | collective-permute-start | bytes 24584 | tf_op jit(solution)/shard_map/ppermute | solution.py:509
  29.2 2.6 %collective-permute-start.4 = (f32[8,256]{1,0:T(8,128)S(1)}, f32[8,256]{1,0:T(8,128)S(1)}, u32[]{:S(2)}, u32[]{:S(2)}) collective-permute-start(f32[8,256]{1,0:T(8,128)S(1)} %get-tuple-element.32), channel_id=1, source_target_pairs={{0,16},{2,18},{4,20},{6,22},{8,24},{10,26},{12,28},{14,30},{16,0},... | collective-permute-start | bytes 24584 | tf_op jit(solution)/shard_map/ppermute | solution.py:509
  31.8 1.3 collective-permute-start.5
  33.7 1.7 collective-permute-done.5
  35.6 3.6 %fusion.15 = (f32[256]{0:T(256)S(1)}, bf16[256,2048]{1,0:T(8,128)(2,1)S(1)}) fusion(bf16[1024,2048]{1,0:T(8,128)(2,1)} %param.16, bf16[256,512]{0,1:T(8,128)(2,1)S(1)} %get-tuple-element.20, bf16[256,512]{0,1:T(8,128)(2,1)S(1)} %get-tuple-element.19, bf16[256,2048]{1,0:T(8,128)(2,1)S(1)} %copy-done.6), kind=kOutput, calls=%fused_computation.18 | convolution fusion | flops 1077935872 | bytes 6816768 | tf_op jit(solution)/shard_map/dot_general | solution.py:476
  39.6 78.5 %dispatch.1 = bf16[4,8,32,2048]{3,2,1,0:T(8,128)(2,1)S(1)} custom-call(bf16[256,2048]{1,0:T(8,128)(2,1)S(1)} %fusion.17.x_ref, f32[4,8,256]{2,1,0:T(8,128)S(1)} %pad_maximum_fusion.3.tab_ref), custom_call_target="tpu_custom_call" | custom-call | tf_op jit(solution)/shard_map/dispatch/pallas_call | solution.py:349
  118.1 4.5 %fusion.5 = f32[1024,1024]{1,0:T(8,128)S(1)} fusion(bf16[1024,2048]{1,0:T(8,128)(2,1)S(1)} %bitcast.74, bf16[1,2048,1024]{2,1,0:T(8,128)(2,1)S(1)} %copy-done.3), kind=kOutput, calls=%fused_computation.8 | convolution fusion | flops 4294967296 | bytes 12582912 | tf_op jit(solution)/shard_map/dot_general | solution.py:398
  122.6 5.3 %multiply_convert_fusion = bf16[1024,1024]{1,0:T(8,128)(2,1)S(1)} fusion(f32[1024,1024]{1,0:T(8,128)S(1)} %fusion.5, bf16[1024,2048]{1,0:T(8,128)(2,1)S(1)} %bitcast.75, bf16[1,2048,1024]{2,1,0:T(8,128)(2,1)S(1)} %copy-done.4), kind=kOutput, calls=%fused_computation.12 | convolution fusion | flops 4301258752 | bytes 14680064 | tf_op jit(solution)/shard_map/dot_general | solution.py:397
  128.0 4.7 %fusion.9 = bf16[1024,2048]{1,0:T(8,128)(2,1)S(1)} fusion(bf16[1024,1024]{1,0:T(8,128)(2,1)S(1)} %multiply_convert_fusion, bf16[1,1024,2048]{2,1,0:T(8,128)(2,1)S(1)} %copy-done.5), kind=kOutput, calls=%fused_computation.13 | convolution fusion | flops 4297064448 | bytes 10485760 | tf_op jit(solution)/shard_map/dot_general | solution.py:400
  132.7 79.8 %combine.1 = bf16[256,2048]{1,0:T(8,128)(2,1)S(1)} custom-call(bf16[4,8,32,2048]{3,2,1,0:T(8,128)(2,1)S(1)} %bitcast.76, f32[4,8,256]{2,1,0:T(8,128)S(1)} %pad_maximum_fusion.3.tab_ref, bf16[256,2048]{1,0:T(8,128)(2,1)S(1)} %get-tuple-element.38.mid_ref), custom_call_target="tpu_custom_call" | custom-call | tf_op jit(solution)/shard_map/combine/pallas_call | solution.py:369
  212.5 1.0 copy.30
  (48 shorter events, 3.2 us)
Async XLA Ops:
  0.0 11.4 %copy-start.1 = (s32[512]{0:T(512)S(1)}, s32[512]{0:T(512)}, u32[]{:S(2)}) copy-start(s32[512]{0:T(512)} %param.14) | copy-start | bytes 6148
  1.9 9.4 %collective-permute-start = (bf16[128,384]{0,1:T(8,128)(2,1)S(1)}, bf16[128,384]{0,1:T(8,128)(2,1)S(1)}, u32[]{:S(2)}, u32[]{:S(2)}) collective-permute-start(bf16[128,384]{0,1:T(8,128)(2,1)S(1)} %get-tuple-element.21), channel_id=1, source_target_pairs={{0,2},{2,4},{4,6},{6,8},{8,10},{10,12},{12,14},{14,16},{16,18},{18... | collective-permute-start | bytes 294920 | tf_op jit(solution)/shard_map/ppermute | solution.py:22
  4.3 7.0 %collective-permute-start.1 = (bf16[128,384]{0,1:T(8,128)(2,1)S(1)}, bf16[128,384]{0,1:T(8,128)(2,1)S(1)}, u32[]{:S(2)}, u32[]{:S(2)}) collective-permute-start(bf16[128,384]{0,1:T(8,128)(2,1)S(1)} %get-tuple-element.22), channel_id=1, source_target_pairs={{2,0},{4,2},{6,4},{8,6},{10,8},{12,10},{14,12},{16,14},{18,16},{20... | collective-permute-start | bytes 294920 | tf_op jit(solution)/shard_map/ppermute | solution.py:24
  17.7 6.4 %copy-start.2 = (f32[256,2]{0,1:T(2,128)S(1)}, f32[256,2]{0,1:T(2,128)}, u32[]{:S(2)}) copy-start(f32[256,2]{0,1:T(2,128)} %param.23) | copy-start | bytes 6148
  17.7 17.9 %copy-start.6 = (bf16[256,2048]{1,0:T(8,128)(2,1)S(1)}, bf16[256,2048]{1,0:T(8,128)(2,1)}, u32[]{:S(2)}) copy-start(bf16[256,2048]{1,0:T(8,128)(2,1)} %param.17) | copy-start | bytes 3145732
  21.7 13.7 %collective-permute-start.2 = (bf16[256,512]{0,1:T(8,128)(2,1)S(1)}, bf16[256,512]{0,1:T(8,128)(2,1)S(1)}, u32[]{:S(2)}, u32[]{:S(2)}) collective-permute-start(bf16[256,512]{0,1:T(8,128)(2,1)S(1)} %constant_dynamic-slice_fusion), channel_id=1, source_target_pairs={{0,1},{1,0},{2,3},{3,2},{4,5},{5,4},{6,7},{7,6},{8,9},{9,8},{10,11... | collective-permute-start | bytes 786440 | tf_op jit(solution)/shard_map/ppermute | solution.py:468
  24.2 8.9 %collective-permute-start.3 = (f32[8,256]{1,0:T(8,128)S(1)}, f32[8,256]{1,0:T(8,128)S(1)}, u32[]{:S(2)}, u32[]{:S(2)}) collective-permute-start(f32[8,256]{1,0:T(8,128)S(1)} %get-tuple-element.32), channel_id=1, source_target_pairs={{0,8},{2,10},{4,12},{6,14},{8,16},{10,18},{12,20},{14,22},{16,24},... | collective-permute-start | bytes 24584 | tf_op jit(solution)/shard_map/ppermute | solution.py:509
  29.2 4.5 %collective-permute-start.4 = (f32[8,256]{1,0:T(8,128)S(1)}, f32[8,256]{1,0:T(8,128)S(1)}, u32[]{:S(2)}, u32[]{:S(2)}) collective-permute-start(f32[8,256]{1,0:T(8,128)S(1)} %get-tuple-element.32), channel_id=1, source_target_pairs={{0,16},{2,18},{4,20},{6,22},{8,24},{10,26},{12,28},{14,30},{16,0},... | collective-permute-start | bytes 24584 | tf_op jit(solution)/shard_map/ppermute | solution.py:509
  31.8 3.7 %collective-permute-start.5 = (f32[8,256]{1,0:T(8,128)S(1)}, f32[8,256]{1,0:T(8,128)S(1)}, u32[]{:S(2)}, u32[]{:S(2)}) collective-permute-start(f32[8,256]{1,0:T(8,128)S(1)} %get-tuple-element.32), channel_id=1, source_target_pairs={{0,24},{2,26},{4,28},{6,30},{8,0},{10,2},{12,4},{14,6},{16,8},{18,... | collective-permute-start | bytes 24584 | tf_op jit(solution)/shard_map/ppermute | solution.py:509
  35.6 3.7 %copy-start = (f32[2048]{0:T(1024)S(1)}, f32[2048]{0:T(1024)}, u32[]{:S(2)}) copy-start(f32[2048]{0:T(1024)} %param.18) | copy-start | bytes 24580
  39.2 78.9 %copy-start.3 = (bf16[1,2048,1024]{2,1,0:T(8,128)(2,1)S(1)}, bf16[1,2048,1024]{2,1,0:T(8,128)(2,1)}, u32[]{:S(2)}) copy-start(bf16[1,2048,1024]{2,1,0:T(8,128)(2,1)} %param.20) | copy-start | bytes 12582916
  118.1 4.5 %copy-start.4 = (bf16[1,2048,1024]{2,1,0:T(8,128)(2,1)S(1)}, bf16[1,2048,1024]{2,1,0:T(8,128)(2,1)}, u32[]{:S(2)}) copy-start(bf16[1,2048,1024]{2,1,0:T(8,128)(2,1)} %param.19) | copy-start | bytes 12582916
  122.6 5.3 %copy-start.5 = (bf16[1,1024,2048]{2,1,0:T(8,128)(2,1)S(1)}, bf16[1,1024,2048]{2,1,0:T(8,128)(2,1)}, u32[]{:S(2)}) copy-start(bf16[1,1024,2048]{2,1,0:T(8,128)(2,1)} %param.21) | copy-start | bytes 12582916

commit v2 on v1

--- a/solution.py
+++ b/solution.py
@@ -10,7 +10,8 @@
 HD = 64
 WIN = 128
 PLANES = 4
-CUTS = 2
+CUTS = 4
+TILE = 256
 MESH = pl.DeviceIdType.MESH
 
 
@@ -69,8 +70,9 @@
 
 def dispatch_kernel(
     planes, stride, tps, cap,
-    x_ref, tab_ref, out_ref,
+    x_ref, tab_ref, gate_ref, up_ref, down_ref, out_ref, tab_out,
     toks, stage, zsend, zrecv, psend, precv, lsem,
+    land, results, hidden, gate_w, up_w, down_w, tabs, tsend, trecv, wsem, ysem,
 ):
     z, r, tp, p = place(stride, tps)
     peers = stride * tps
@@ -105,7 +107,7 @@
     def plane_copy(zs, h, dest, at):
         return pltpu.make_async_remote_copy(
             src_ref=stage.at[zs, pl.ds(pl.multiple_of(dest * cap, cap), cap), span(h)],
-            dst_ref=out_ref.at[zs, at, :, span(h)],
+            dst_ref=land.at[zs, pl.ds(pl.multiple_of(at * cap, cap), cap), span(h)],
             send_sem=psend.at[zs, h, dest],
             recv_sem=precv.at[zs, h, at],
             device_id=(z * stride + lax.div(dest, tps), lax.rem(dest, tps)),
@@ -115,13 +117,65 @@
     def local_copy(zs, h):
         return pltpu.make_async_copy(
             stage.at[zs, pl.ds(pl.multiple_of(p * cap, cap), cap), span(h)],
-            out_ref.at[zs, p, :, span(h)],
+            land.at[zs, pl.ds(pl.multiple_of(p * cap, cap), cap), span(h)],
             lsem.at[zs, h],
         )
 
+    def tab_hop(zs, side, source):
+        return pltpu.make_async_remote_copy(
+            src_ref=source,
+            dst_ref=tabs.at[zs],
+            send_sem=tsend.at[side, zs],
+            recv_sem=trecv.at[zs],
+            device_id=((z + 1 - 2 * side) * stride + r, tp),
+            device_id_type=MESH,
+        )
+
+    loads = [
+        pltpu.make_async_copy(source, target, wsem.at[k])
+        for k, (source, target) in enumerate(
+            [(gate_ref, gate_w), (up_ref, up_w), (down_ref, down_w)]
+        )
+    ]
+
+    def result_copy(zs):
+        return pltpu.make_async_copy(results.at[zs], out_ref.at[zs], ysem.at[zs])
+
+    def experts(zs):
+        @pl.loop(0, CUTS)
+        def _(h):
+            local_copy(zs, h).wait()
+            for k in range(1, peers):
+                other = lax.rem(p + k, peers)
+                plane_copy(zs, h, other, other).wait_recv()
+
+        @pl.loop(0, gate_w.shape[1] // TILE)
+        def _(c):
+            at = pl.ds(pl.multiple_of(c * TILE, TILE), TILE)
+            gate = jnp.dot(land[zs], gate_w[:, at], preferred_element_type=jnp.float32)
+            upper = jnp.dot(land[zs], up_w[:, at], preferred_element_type=jnp.float32)
+            hidden[:, at] = (gate / (1.0 + jnp.exp(-gate)) * upper).astype(jnp.bfloat16)
+
+        @pl.loop(0, width // TILE)
+        def _(c):
+            at = pl.ds(pl.multiple_of(c * TILE, TILE), TILE)
+            results[zs, :, at] = jnp.dot(
+                hidden[...], down_w[:, at], preferred_element_type=jnp.float32
+            ).astype(jnp.bfloat16)
+
+        result_copy(zs).start()
+
+    def experts_at(dist):
+        @pl.loop(0, 2)
+        def _(side):
+            zs = z - dist + 2 * dist * side
+
+            @pl.when((zs >= 0) & (zs < planes) & ((dist > 0) | (side == 0)))
+            def _():
+                experts(zs)
+
     def pack(block, zs, h):
-        tab = tab_ref[lax.rem(z - zs + planes, planes)]
-        first, second = slot_hits(tab, z, slots, rows)
+        first, second = slot_hits(tabs[zs], z, slots, rows)
         pick = jnp.where(first | second, 1.0, 0.0).astype(jnp.bfloat16)
         stage[zs, :, span(h)] = jnp.dot(
             pick, block, preferred_element_type=jnp.float32
@@ -130,6 +184,14 @@
             plane_copy(zs, h, lax.rem(p + k, peers), p).start()
         local_copy(zs, h).start()
 
+    @pl.when(z < planes - 1)
+    def _():
+        tab_hop(z, 0, tab_ref).start()
+
+    @pl.when(z > 0)
+    def _():
+        tab_hop(z, 1, tab_ref).start()
+
     for h in range(CUTS):
 
         @pl.when(z < planes - 1)
@@ -139,10 +201,17 @@
         @pl.when(z > 0)
         def _():
             own_hop(h, 1).start()
+
+    for load in loads:
+        load.start()
+    tabs[z] = tab_ref[...]
 
     @pl.loop(0, CUTS)
     def _(h):
         pack(x_ref[:, span(h)], z, h)
+
+    for load in loads:
+        load.wait()
 
     @pl.loop(0, 2 * CUTS * (planes - 1))
     def _(e):
@@ -153,14 +222,29 @@
 
         @pl.when((zs >= 0) & (zs < planes))
         def _():
+            onward = z + 1 - 2 * side
+
+            @pl.when(h == 0)
+            def _():
+                tab_hop(zs, side, tabs.at[zs]).wait_recv()
+
+                @pl.when((onward >= 0) & (onward < planes))
+                def _():
+                    tab_hop(zs, side, tabs.at[zs]).start()
+
             hop(zs, h, side).wait_recv()
-            onward = z + 1 - 2 * side
 
             @pl.when((onward >= 0) & (onward < planes))
             def _():
                 hop(zs, h, side).start()
 
             pack(toks[zs, :, span(h)], zs, h)
+
+        @pl.when((side == 1) & (h == CUTS // 2 - 1))
+        def _():
+            experts_at(dist - 1)
+
+    experts_at(planes - 1)
 
     @pl.loop(0, planes * CUTS)
     def _(e):
@@ -175,11 +259,22 @@
         def _():
             hop(zs, h, 1).wait_send()
 
-        local_copy(zs, h).wait()
         for k in range(1, peers):
-            other = lax.rem(p + k, peers)
-            plane_copy(zs, h, other, p).wait_send()
-            plane_copy(zs, h, other, other).wait_recv()
+            plane_copy(zs, h, lax.rem(p + k, peers), p).wait_send()
+
+    @pl.loop(0, planes)
+    def _(zs):
+        @pl.when((zs <= z) & (z < planes - 1))
+        def _():
+            tab_hop(zs, 0, tabs.at[zs]).wait_send()
+
+        @pl.when((zs >= z) & (z > 0))
+        def _():
+            tab_hop(zs, 1, tabs.at[zs]).wait_send()
+
+        result_copy(zs).wait()
+
+    tab_out[...] = tabs[...]
 
 
 def return_kernel(
@@ -199,7 +294,7 @@
 
     def plane_copy(zs, h, dest, at):
         return pltpu.make_async_remote_copy(
-            src_ref=y_ref.at[zs, dest, :, span(h)],
+            src_ref=y_ref.at[zs, pl.ds(pl.multiple_of(dest * cap, cap), cap), span(h)],
             dst_ref=held.at[zs, pl.ds(pl.multiple_of(at * cap, cap), cap), span(h)],
             send_sem=psend.at[zs, h, dest],
             recv_sem=precv.at[zs, h, at],
@@ -209,7 +304,7 @@
 
     def local_copy(zs, h):
         return pltpu.make_async_copy(
-            y_ref.at[zs, p, :, span(h)],
+            y_ref.at[zs, pl.ds(pl.multiple_of(p * cap, cap), cap), span(h)],
             held.at[zs, pl.ds(pl.multiple_of(p * cap, cap), cap), span(h)],
             lsem.at[zs, h],
         )
@@ -243,7 +338,7 @@
         local_copy(zs, h).wait()
         for k in range(1, peers):
             plane_copy(zs, h, p, lax.rem(p + k, peers)).wait_recv()
-        tab = tab_ref[lax.rem(z - zs + planes, planes)]
+        tab = tab_ref[zs]
         first, second = slot_hits(tab, z, slots, rows)
         mix = jnp.where(first, tab[2:3, :], 0.0) + jnp.where(second, tab[3:4, :], 0.0)
         return jnp.dot(
@@ -337,8 +432,7 @@
             plane_copy(zs, h, lax.rem(p + k, peers), p).wait_send()
 
 
-def routed_by_plane(normed, mid, tables, cap, weights):
-    planes = tables.shape[0]
+def routed_by_plane(normed, mid, tab, planes, cap, weights):
     rows, width = normed.shape
     tps = lax.axis_size("tp")
     stride = lax.axis_size("sp") // planes
@@ -346,11 +440,15 @@
     dma = pltpu.SemaphoreType.DMA
     vmem = pl.BlockSpec(memory_space=pltpu.VMEM)
     anywhere = pl.BlockSpec(memory_space=pl.ANY)
-    arrived = pl.pallas_call(
+    hidden = weights[0].shape[1]
+    finished, tables = pl.pallas_call(
         functools.partial(dispatch_kernel, planes, stride, tps, cap),
-        out_shape=jax.ShapeDtypeStruct((planes, peers, cap, width), jnp.bfloat16),
-        in_specs=[vmem, vmem],
-        out_specs=anywhere,
+        out_shape=[
+            jax.ShapeDtypeStruct((planes, peers * cap, width), jnp.bfloat16),
+            jax.ShapeDtypeStruct((planes,) + tab.shape, jnp.float32),
+        ],
+        in_specs=[vmem, vmem, anywhere, anywhere, anywhere],
+        out_specs=[anywhere, vmem],
         scratch_shapes=[
             pltpu.VMEM((planes, rows, width), jnp.bfloat16),
             pltpu.VMEM((planes, peers * cap, width), jnp.bfloat16),
@@ -359,13 +457,23 @@
             dma((planes, CUTS, peers)),
             dma((planes, CUTS, peers)),
             dma((planes, CUTS)),
+            pltpu.VMEM((planes, peers * cap, width), jnp.bfloat16),
+            pltpu.VMEM((planes, peers * cap, width), jnp.bfloat16),
+            pltpu.VMEM((peers * cap, hidden), jnp.bfloat16),
+            pltpu.VMEM((width, hidden), jnp.bfloat16),
+            pltpu.VMEM((width, hidden), jnp.bfloat16),
+            pltpu.VMEM((hidden, width), jnp.bfloat16),
+            pltpu.VMEM((planes,) + tab.shape, jnp.float32),
+            dma((2, planes)),
+            dma((planes,)),
+            dma((3,)),
+            dma((planes,)),
         ],
         compiler_params=pltpu.CompilerParams(
-            collective_id=0, has_side_effects=True, vmem_limit_bytes=32 * 1024 * 1024
+            collective_id=0, has_side_effects=True, vmem_limit_bytes=48 * 1024 * 1024
         ),
         name="dispatch",
-    )(normed, tables)
-    finished = expert_rows(arrived, *weights)
+    )(normed, tab, *weights)
     return pl.pallas_call(
         functools.partial(return_kernel, planes, stride, tps, cap),
         out_shape=jax.ShapeDtypeStruct((rows, width), jnp.bfloat16),
@@ -502,20 +610,11 @@
             ],
             axis=0,
         )
-        stride = sp_count // PLANES
-        tables = jnp.stack(
-            [tab]
-            + [
-                lax.ppermute(
-                    tab, "sp", [(i, (i + d * stride) % sp_count) for i in range(sp_count)]
-                )
-                for d in range(1, PLANES)
-            ]
-        )
         return routed_by_plane(
             normed,
             mid_wide.astype(jnp.bfloat16),
-            tables,
+            tab,
+            PLANES,
             capacity,
             (expert_gate[0], expert_up[0], expert_down[0]),
         )

time: 214 us -> 204 us (0.953)
  matrix products: 24.2 us -> 9.69 us
  Pallas kernels: 158 us -> 169 us
  starting transfers between devices: 15 us -> 6.07 us
  waiting for transfers between devices: 2.31 us -> 5.09 us
    dot_general x3 -> x0, matrix products: 14.5 us -> none  [the longest x1 5.31 us: expert_rows(): gate = jnp.dot(flat_rows, gate_w, preferred_element_type=jnp.float32)]
    pallas_call x1, Pallas kernels: 78.5 us -> 90.4 us  [routed_by_plane(): pl.pallas_call(functools.partial(dispatch_kernel, planes, stride, tps, ca...]
    ppermute x3 -> x0, starting transfers between devices: 8.93 us -> none  [shards(): lax.ppermute(tab, 'sp', [(i, (i + d * stride) % sp_count) for i in range(...]
    ppermute x1, waiting for transfers between devices: 0.01 us -> 5.07 us  [shards(): lax.ppermute(lax.dynamic_slice_in_dim(attended, (1 - tp) * half, half, 0)...]
    ppermute x3 -> x0, waiting for transfers between devices: 2.3 us -> none  [shards(): lax.ppermute(tab, 'sp', [(i, (i + d * stride) % sp_count) for i in range(...]
  transfers between devices with their start and end apart: 6 -> 3, of which waited for: 2 -> 1; matrix products, arithmetic and copies ran while one was open for 3% -> 2% of each run, Pallas kernels for 0% -> 0%
where the time goes in v2:
time: 204 us; the launch traced here: 203 us
  Pallas kernels  169 us (83%)
  matrix products  9.69 us (5%)
  other arithmetic  6.79 us (3%)
  starting transfers between devices  6.07 us (3%)
  local copies, waits for them, and re-layouts  5.8 us (3%)
  waiting for transfers between devices  5.09 us (2%)
    pallas_call x1, Pallas kernels, routed_by_plane(): pl.pallas_call(functools.partial(dispatch_kernel, planes, stride, tps, ca...  90.4 us
    pallas_call x1, Pallas kernels, routed_by_plane(): pl.pallas_call(functools.partial(return_kernel, planes, stride, tps, cap)...  79 us
    ppermute x1, waiting for transfers between devices, shards(): lax.ppermute(lax.dynamic_slice_in_dim(attended, (1 - tp) * half, half, 0)...  5.07 us
  transfers between devices with their start and end apart: 3, of which 1 were waited for; matrix products, arithmetic and copies ran while one was open for 2% of the time, Pallas kernels for 0%

profile of v2, /device:TPU:0, one launch (start us, length us, event | category | flops | bytes accessed | tf_op | source)
XLA Modules:
  0.0 203.1 jit_solution(16920553727962454942)
XLA Ops:
  0.0 1.1 copy.26
  1.1 0.7 convert_element_type.46
  1.9 2.4 %collective-permute-start = (bf16[128,384]{0,1:T(8,128)(2,1)S(1)}, bf16[128,384]{0,1:T(8,128)(2,1)S(1)}, u32[]{:S(2)}, u32[]{:S(2)}) collective-permute-start(bf16[128,384]{0,1:T(8,128)(2,1)S(1)} %get-tuple-element.34), channel_id=1, source_target_pairs={{0,2},{2,4},{4,6},{6,8},{8,10},{10,12},{12,14},{14,16},{16,18},{18... | collective-permute-start | bytes 294920 | tf_op jit(solution)/shard_map/ppermute | solution.py:23
  4.3 1.3 collective-permute-start.1
  5.6 0.8 copy.19
  6.4 0.1 eq.57
  6.5 0.1 eq.53
  6.7 1.3 copy.17
  8.0 0.7 max.22
  8.7 1.2 reduce-window.6
  9.9 0.2 slice_reduce_fusion
  10.3 0.1 sub.66
  10.7 0.9 fusion.8
  11.6 2.1 %fusion = (f32[2,4,512]{2,1,0:T(4,128)S(1)}, f32[2,768,512,4]{2,1,3,0:T(8,128)S(1)}) fusion(pred[512,768]{0,1:T(8,128)(4,1)S(1)} %fusion.8, bf16[512,2,4,64]{0,3,2,1:T(8,128)(2,1)S(1)} %bitcast.60, bf16[768,2,128]{0,2,1:T(8,128)(2,1)S(1)} %bitcast.61), kind=kOutput, calls=%fused_computation.3 | convolution fusion | flops 412086272 | bytes 13713408 | tf_op jit(solution)/shard_map/while/body/eval_jaxpr/qhgd,khd->hgqk/dot_general | solution.py:548
  13.7 3.1 %fusion.1 = f32[2,4,512]{2,1,0:T(4,128)S(1)} fusion(f32[2,768,512,4]{2,1,3,0:T(8,128)S(1)} %get-tuple-element.38, f32[2,4,512]{2,1,0:T(4,128)S(1)} %broadcast_maximum_fusion, pred[512,768]{0,1:T(8,128)(4,1)S(1)} %fusion.8), kind=kLoop, calls=%fused_computation.4 | loop fusion | flops 15724544 | bytes 13008896 | tf_op jit(solution)/shard_map/while/body/eval_jaxpr/reduce_sum | solution.py:562
  16.9 4.0 %fusion.9 = bf16[2,64,4,512]{3,1,2,0:T(8,128)(2,1)S(1)} fusion(f32[2,768,512,4]{2,1,3,0:T(8,128)S(1)} %get-tuple-element.38, f32[2,4,512]{2,1,0:T(4,128)S(1)} %exponential_add_fusion, f32[2,4,512]{2,1,0:T(4,128)S(1)} %broadcast_maximum_fusion, pred[512,768]{0,1:T(8,128)(4,1)S(1)} %fusion.8, bf16[768,2,128]{0,2,1:T(8,128)(2,1)S(1)} %bitcast.62), kind=kOutput, calls=%fused_computation.16 | convolution fusion | flops 421789696 | bytes 13729792 | tf_op jit(solution)/shard_map/while/body/eval_jaxpr/hgqk,khd->qhgd/dot_general | solution.py:564
  21.0 2.4 %collective-permute-start.2 = (bf16[256,512]{0,1:T(8,128)(2,1)S(1)}, bf16[256,512]{0,1:T(8,128)(2,1)S(1)}, u32[]{:S(2)}, u32[]{:S(2)}) collective-permute-start(bf16[256,512]{0,1:T(8,128)(2,1)S(1)} %constant_dynamic-slice_fusion), channel_id=1, source_target_pairs={{0,1},{1,0},{2,3},{3,2},{4,5},{5,4},{6,7},{7,6},{8,9},{9,8},{10,11... | collective-permute-start | bytes 786440 | tf_op jit(solution)/shard_map/ppermute | solution.py:576
  23.5 5.1 %collective-permute-done.2 = bf16[256,512]{0,1:T(8,128)(2,1)S(1)} collective-permute-done((bf16[256,512]{0,1:T(8,128)(2,1)S(1)}, bf16[256,512]{0,1:T(8,128)(2,1)S(1)}, u32[]{:S(2)}, u32[]{:S(2)}) %collective-permute-start.2) | collective-permute-done | bytes 262176 | tf_op jit(solution)/shard_map/ppermute | solution.py:576
  28.6 0.1 broadcast_select_fusion.1
  28.7 3.6 %fusion.4 = (f32[256]{0:T(256)S(1)}, bf16[256,2048]{1,0:T(8,128)(2,1)S(1)}) fusion(bf16[1024,2048]{1,0:T(8,128)(2,1)} %param.16, bf16[256,512]{0,1:T(8,128)(2,1)S(1)} %get-tuple-element.32, bf16[256,512]{0,1:T(8,128)(2,1)S(1)} %get-tuple-element.23, bf16[256,2048]{1,0:T(8,128)(2,1)S(1)} %copy-done.4), kind=kOutput, calls=%fused_computation.10 | convolution fusion | flops 1077935872 | bytes 6816768 | tf_op jit(solution)/shard_map/dot_general | solution.py:584
  32.4 0.3 fusion.6.x_ref
  32.7 90.4 %dispatch.1 = (bf16[4,256,2048]{2,1,0:T(8,128)(2,1)S(1)}, f32[4,8,256]{2,1,0:T(8,128)S(1)}) custom-call(bf16[256,2048]{1,0:T(8,128)(2,1)S(1)} %fusion.6.x_ref, f32[8,256]{1,0:T(8,128)S(1)} %maximum_maximum_fusion.tab_ref, bf16[2048,1024]{1,0:T(8,128)(2,1)} %bitcast.54, bf16[2048,1024]{1,0:T(8,128)(2,1)} %bitcast.55, bf16[1024,2048]{1,0:T(8,128)(2,1)} %bitcast.56), custom_call_target="tpu_custom_call" | custom-call | tf_op jit(solution)/shard_map/dispatch/pallas_call | solution.py:444
  123.1 79.0 %combine.1 = bf16[256,2048]{1,0:T(8,128)(2,1)S(1)} custom-call(bf16[4,256,2048]{2,1,0:T(8,128)(2,1)S(1)} %get-tuple-element.21.y_ref, f32[4,8,256]{2,1,0:T(8,128)S(1)} %get-tuple-element.22.tab_ref, bf16[256,2048]{1,0:T(8,128)(2,1)S(1)} %get-tuple-element.40.mid_ref), custom_call_target="tpu_custom_call" | custom-call | tf_op jit(solution)/shard_map/combine/pallas_call | solution.py:477
  202.2 1.0 copy.30
  (34 shorter events, 0.8 us)
Async XLA Ops:
  0.0 10.7 %copy-start.2 = (s32[512]{0:T(512)S(1)}, s32[512]{0:T(512)}, u32[]{:S(2)}) copy-start(s32[512]{0:T(512)} %param.14) | copy-start | bytes 6148
  1.9 8.7 %collective-permute-start = (bf16[128,384]{0,1:T(8,128)(2,1)S(1)}, bf16[128,384]{0,1:T(8,128)(2,1)S(1)}, u32[]{:S(2)}, u32[]{:S(2)}) collective-permute-start(bf16[128,384]{0,1:T(8,128)(2,1)S(1)} %get-tuple-element.34), channel_id=1, source_target_pairs={{0,2},{2,4},{4,6},{6,8},{8,10},{10,12},{12,14},{14,16},{16,18},{18... | collective-permute-start | bytes 294920 | tf_op jit(solution)/shard_map/ppermute | solution.py:23
  4.3 6.3 %collective-permute-start.1 = (bf16[128,384]{0,1:T(8,128)(2,1)S(1)}, bf16[128,384]{0,1:T(8,128)(2,1)S(1)}, u32[]{:S(2)}, u32[]{:S(2)}) collective-permute-start(bf16[128,384]{0,1:T(8,128)(2,1)S(1)} %get-tuple-element.36), channel_id=1, source_target_pairs={{2,0},{4,2},{6,4},{8,6},{10,8},{12,10},{14,12},{16,14},{18,16},{20... | collective-permute-start | bytes 294920 | tf_op jit(solution)/shard_map/ppermute | solution.py:25
  16.9 6.4 %copy-start.1 = (s32[256,2]{0,1:T(2,128)S(1)}, s32[256,2]{0,1:T(2,128)}, u32[]{:S(2)}) copy-start(s32[256,2]{0,1:T(2,128)} %param.22) | copy-start | bytes 6148
  16.9 6.5 %copy-start.3 = (f32[256,2]{0,1:T(2,128)S(1)}, f32[256,2]{0,1:T(2,128)}, u32[]{:S(2)}) copy-start(f32[256,2]{0,1:T(2,128)} %param.23) | copy-start | bytes 6148
  16.9 11.8 %copy-start.4 = (bf16[256,2048]{1,0:T(8,128)(2,1)S(1)}, bf16[256,2048]{1,0:T(8,128)(2,1)}, u32[]{:S(2)}) copy-start(bf16[256,2048]{1,0:T(8,128)(2,1)} %param.17) | copy-start | bytes 3145732
  21.0 7.6 %collective-permute-start.2 = (bf16[256,512]{0,1:T(8,128)(2,1)S(1)}, bf16[256,512]{0,1:T(8,128)(2,1)S(1)}, u32[]{:S(2)}, u32[]{:S(2)}) collective-permute-start(bf16[256,512]{0,1:T(8,128)(2,1)S(1)} %constant_dynamic-slice_fusion), channel_id=1, source_target_pairs={{0,1},{1,0},{2,3},{3,2},{4,5},{5,4},{6,7},{7,6},{8,9},{9,8},{10,11... | collective-permute-start | bytes 786440 | tf_op jit(solution)/shard_map/ppermute | solution.py:576
  28.7 3.6 %copy-start = (f32[2048]{0:T(1024)S(1)}, f32[2048]{0:T(1024)}, u32[]{:S(2)}) copy-start(f32[2048]{0:T(1024)} %param.18) | copy-start | bytes 24580
